TPU v7x, 32 devices: a whole 2x2x4 slice. The times are simulated.
32 devices in a mesh: rep: 2 (over x), fs: 8 (over z, y), tp: 2 (over core).
Axes of the slice: x: 2, y: 2, z: 4, core: 2. Of those that a mesh axis runs over, the one named last changes fastest.
Arguments:
- tokens: bfloat16 [16, 64, 2048], P(('rep', 'fs'), None, 'tp'), may hold values from -6 to 6
- lin_weight: bfloat16 [2048, 1024], P('fs', 'tp'), may hold values from -0.125 to 0.125
- glu_weight: bfloat16 [2048, 1024], P('fs', 'tp'), may hold values from -0.125 to 0.125
- conv_taps: float32 [31, 1024], P(None, 'tp'), may hold values from -4 to 4
- conv_gain: float32 [1024], P('tp'), may hold values from 0.1 to 1.9
- conv_out_weight: bfloat16 [1024, 2048], P('tp', 'fs'), may hold values from -0.1875 to 0.1875
- mix_gain: float32 [2048], replicated, may hold values from 0.1 to 1.9
- ff_gate: bfloat16 [2048, 5632], P('fs', 'tp'), may hold values from -0.125 to 0.125
- ff_up: bfloat16 [2048, 5632], P('fs', 'tp'), may hold values from -0.125 to 0.125
- ff_down: bfloat16 [5632, 2048], P('tp', 'fs'), may hold values from -0.078125 to 0.078125
- out_gain: float32 [2048], replicated, may hold values from 0.1 to 1.9
Outputs:
- encoded: bfloat16 [16, 64, 2048], P(('rep', 'fs'), None, 'tp')
All inputs are finite; a program needn't handle non-finite values.
Results may differ from a plain program's by a relative error of at most 0.014.
Values may be sent and summed in bfloat16 or wider, within the bound.
No kernel may reach another device: no remote copies, remote signals or barrier semaphores. Data moves between devices by JAX's collectives and lax.ppermute only.
A program may use at most 128 MiB of HBM per device.

v0:
```python
import jax
import jax.numpy as jnp
from jax import lax
from jax.sharding import PartitionSpec as P

D = 2048
CONV = 1024
TAPS = 31


residual_scale = 2.0**0.25
epsilon = 1e-05


def rounded(value):
    return lax.optimization_barrier(value.astype(jnp.bfloat16)).astype(jnp.float32)


def scaled(values, totals, squares, count):
    average = totals[:, None] / count
    second = squares[:, None] / count
    return (values - average) * lax.rsqrt(second - average * average + epsilon)


def on_device(
    tokens,
    lin_weight,
    glu_weight,
    conv_taps,
    conv_gain,
    conv_out_weight,
    mix_gain,
    ff_gate,
    ff_up,
    ff_down,
    out_gain,
):
    own_tokens = tokens[0]
    feat_width = own_tokens.shape[1]
    offset = lax.axis_index("tp") * feat_width
    all_tokens = lax.all_gather(own_tokens, "tp", axis=1, tiled=True)
    seq_rows = all_tokens.shape[0]
    pieces = (
        lax.all_gather(lin_weight, "fs", axis=0, tiled=True),
        lax.all_gather(glu_weight, "fs", axis=0, tiled=True),
    )
    columns = all_tokens
    linear = jnp.dot(columns, pieces[0], preferred_element_type=jnp.float32)
    gating = jnp.dot(columns, pieces[1], preferred_element_type=jnp.float32)
    glu = (linear * jax.nn.sigmoid(gating)).astype(jnp.bfloat16)
    margin = (TAPS - 1) // 2
    conv = lax.conv_general_dilated(
        glu.astype(jnp.float32)[None],
        conv_taps[:, None, :],
        (1,),
        [(margin, margin)],
        dimension_numbers=("NWC", "WIO", "NWC"),
        feature_group_count=glu.shape[1],
        precision=lax.Precision.HIGHEST,
    )[0]
    conv_sums, conv_squares = lax.psum((jnp.sum(conv, axis=1), jnp.sum(conv * conv, axis=1)), "tp")
    activated = jax.nn.silu(scaled(conv, conv_sums, conv_squares, CONV) * conv_gain).astype(
        jnp.bfloat16
    )
    conv_terms = jnp.dot(
        activated,
        lax.all_gather(conv_out_weight, "fs", axis=1, tiled=True),
        preferred_element_type=jnp.float32,
    )
    mixed = rounded(
        lax.psum_scatter(
            conv_terms.astype(jnp.bfloat16), "tp", scatter_dimension=1, tiled=True
        ).astype(jnp.float32)
    )
    before = residual_scale * own_tokens.astype(jnp.float32) + mixed
    mix_sums, mix_squares = lax.psum(
        (jnp.sum(before, axis=1), jnp.sum(before * before, axis=1)), "tp"
    )
    gain_own = lax.dynamic_slice_in_dim(mix_gain, offset, feat_width, 0)
    middle_own = (scaled(before, mix_sums, mix_squares, D) * gain_own).astype(jnp.bfloat16)
    middle_all = lax.all_gather(middle_own, "tp", axis=1, tiled=True)
    empty_ffn = jnp.zeros((seq_rows, ff_gate.shape[1]), jnp.float32)
    pieces = (
        lax.all_gather(ff_gate, "fs", axis=0, tiled=True),
        lax.all_gather(ff_up, "fs", axis=0, tiled=True),
    )
    columns = lax.slice_in_dim(middle_all, 0, pieces[0].shape[0], axis=1)
    gate = empty_ffn + jnp.dot(columns, pieces[0], preferred_element_type=jnp.float32)
    upward = empty_ffn + jnp.dot(columns, pieces[1], preferred_element_type=jnp.float32)
    hidden = (jax.nn.silu(gate) * upward).astype(jnp.bfloat16)
    down_terms = jnp.dot(
        hidden,
        lax.all_gather(ff_down, "fs", axis=1, tiled=True),
        preferred_element_type=jnp.float32,
    )
    forward = rounded(
        lax.psum_scatter(
            down_terms.astype(jnp.bfloat16), "tp", scatter_dimension=1, tiled=True
        ).astype(jnp.float32)
    )
    final = residual_scale * middle_own.astype(jnp.float32) + forward
    out_sums, out_squares = lax.psum((jnp.sum(final, axis=1), jnp.sum(final * final, axis=1)), "tp")
    gain_slice = lax.dynamic_slice_in_dim(out_gain, offset, feat_width, 0)
    encoded = (scaled(final, out_sums, out_squares, D) * gain_slice).astype(jnp.bfloat16)
    return encoded[None]


def solution(mesh):
    return jax.shard_map(
        on_device,
        mesh=mesh,
        in_specs=(
            P(("rep", "fs"), None, "tp"),
            P("fs", "tp"),
            P("fs", "tp"),
            P(None, "tp"),
            P("tp"),
            P("tp", "fs"),
            P(),
            P("fs", "tp"),
            P("fs", "tp"),
            P("tp", "fs"),
            P(),
        ),
        out_specs=P(("rep", "fs"), None, "tp"),
        check_vma=False,
    )
```

profile of v0, /device:TPU:0, one launch (start us, length us, event | category | flops | bytes accessed | tf_op | source)
XLA Modules:
  0.0 695.2 jit_solution(6831628930254306742)
XLA Ops:
  6.5 0.7 all-gather.8.cloned.1.call-update
  8.8 2.3 all-gather
  11.1 50.2 %all-gather.8.cloned.1.call-done = bf16[2048,512]{1,0:T(8,128)(2,1)} async-done(((bf16[256,512]{1,0:T(8,128)(2,1)}), bf16[2048,512]{1,0:T(8,128)(2,1)}) %all-gather.8.cloned.1.call-update) | async-done | bytes 2097168 | tf_op jit(solution)/shard_map/all_gather | solution.py:44
  61.3 2.1 fusion.9
  63.4 47.7 %all-gather.10.cloned.1.call-done = bf16[2048,512]{1,0:T(8,128)(2,1)} async-done(((bf16[256,512]{1,0:T(8,128)(2,1)}), bf16[2048,512]{1,0:T(8,128)(2,1)}) %all-gather.10.cloned.1.call-update) | async-done | bytes 2097168 | tf_op jit(solution)/shard_map/all_gather | solution.py:45
  111.1 2.1 fusion.6
  113.2 1.3 fusion.26
  114.6 2.5 all-reduce.2
  117.1 44.9 %all-gather.12.cloned.1.call-done = bf16[512,2048]{1,0:T(8,128)(2,1)} async-done(((bf16[512,256]{1,0:T(8,128)(2,1)}), bf16[512,2048]{1,0:T(8,128)(2,1)}) %all-gather.12.cloned.1.call-update) | async-done | bytes 2097168 | tf_op jit(solution)/shard_map/all_gather | solution.py:67
  162.0 2.8 convolution_convert_fusion.1
  166.9 4.1 reduce-scatter.3.cloned.1.call-done
  171.0 1.1 fusion.12
  172.1 2.5 all-reduce.1
  174.5 1.0 multiply_convert_fusion.1
  175.5 2.0 all_gather.28
  177.5 159.9 %all-gather.14.cloned.1.call-done = bf16[2048,2816]{1,0:T(8,128)(2,1)} async-done(((bf16[256,2816]{1,0:T(8,128)(2,1)}), bf16[2048,2816]{1,0:T(8,128)(2,1)}) %all-gather.14.cloned.1.call-update) | async-done | bytes 11534352 | tf_op jit(solution)/shard_map/all_gather | solution.py:84
  337.5 6.3 fusion.27
  343.9 157.2 %all-gather.16.cloned.1.call-done = bf16[2048,2816]{1,0:T(8,128)(2,1)} async-done(((bf16[256,2816]{1,0:T(8,128)(2,1)}), bf16[2048,2816]{1,0:T(8,128)(2,1)}) %all-gather.16.cloned.1.call-update) | async-done | bytes 11534352 | tf_op jit(solution)/shard_map/all_gather | solution.py:85
  501.1 163.6 %all-gather.18.cloned.1.call-done = bf16[2816,2048]{1,0:T(8,128)(2,1)} async-done(((bf16[2816,256]{1,0:T(8,128)(2,1)}), bf16[2816,2048]{1,0:T(8,128)(2,1)}) %all-gather.18.cloned.1.call-update) | async-done | bytes 11534352 | tf_op jit(solution)/shard_map/all_gather | solution.py:93
  664.6 12.4 %convolution_convert_fusion = bf16[64,2048]{1,0:T(8,128)(2,1)} fusion(bf16[2816,2048]{1,0:T(8,128)(2,1)} %all-gather.18.cloned.1.call-done, bf16[64,2048]{1,0:T(8,128)(2,1)S(1)} %all_gather.28, bf16[2048,2816]{1,0:T(8,128)(2,1)} %all-gather.16.cloned.1.call-done, f32[64,2816]{1,0:T(8,128)S(1)} %fusion.27), kind=kOutput, calls=%fused_computation.2 | convolution fusion | flops 1477607424 | bytes 24313856 | tf_op jit(solution)/shard_map/dot_general | solution.py:91
  677.0 6.1 reduce-scatter.5.cloned.1.call-done
  683.1 1.1 fusion.11
  684.2 2.5 all-reduce
  686.6 1.7 fusion.13
  (30 shorter events, 3.6 us)
Async XLA Ops:
  6.5 106.6 %copy-start = (f32[31,512]{1,0:T(8,128)S(1)}, f32[31,512]{1,0:T(8,128)}, u32[]{:S(2)}) copy-start(f32[31,512]{1,0:T(8,128)} %param.14) | copy-start | bytes 190468
  6.5 54.8 %all-gather.8.cloned.1.call-start = ((), (), s32[]{:S(2)}) async-start(), calls=%async_computation.2 | async-start | bytes 2359296 | tf_op jit(solution)/shard_map/all_gather | solution.py:44
  7.3 103.8 %all-gather.10.cloned.1.call-start = ((), (), s32[]{:S(2)}) async-start(), calls=%async_computation.3 | async-start | bytes 2359296 | tf_op jit(solution)/shard_map/all_gather | solution.py:45
  8.0 154.0 %all-gather.12.cloned.1.call-start = ((), (), s32[]{:S(2)}) async-start(), calls=%async_computation.4 | async-start | bytes 2359296 | tf_op jit(solution)/shard_map/all_gather | solution.py:67
  8.7 162.2 %reduce-scatter.3.cloned.1.call-start = ((), (), s32[]{:S(2)}) async-start(), calls=%async_computation.5 | async-start | bytes 393216 | tf_op jit(solution)/shard_map/reduce_scatter | solution.py:71
  63.4 98.7 %copy-start.3 = (f32[512]{0:T(512)S(1)}, f32[512]{0:T(512)}, u32[]{:S(2)}) copy-start(f32[512]{0:T(512)} %param.15) | copy-start | bytes 6148
  164.9 2.0 copy-start.2
  164.9 6.1 copy-start.1
  164.9 172.6 %all-gather.14.cloned.1.call-start = ((), (), s32[]{:S(2)}) async-start(), calls=%async_computation.6 | async-start | bytes 12976128 | tf_op jit(solution)/shard_map/all_gather | solution.py:84
  165.5 335.5 %all-gather.16.cloned.1.call-start = ((), (), s32[]{:S(2)}) async-start(), calls=%async_computation.7 | async-start | bytes 12976128 | tf_op jit(solution)/shard_map/all_gather | solution.py:85
  166.1 498.5 %all-gather.18.cloned.1.call-start = ((), (), s32[]{:S(2)}) async-start(), calls=%async_computation.8 | async-start | bytes 12976128 | tf_op jit(solution)/shard_map/all_gather | solution.py:93
  166.8 516.3 %reduce-scatter.5.cloned.1.call-start = ((), (), s32[]{:S(2)}) async-start(), calls=%async_computation.9 | async-start | bytes 393216 | tf_op jit(solution)/shard_map/reduce_scatter | solution.py:97
  343.8 342.8 %dynamic-slice-start = ((f32[2048]{0:T(1024)}, s32[]{:T(128)}), f32[1024]{0:T(1024)S(1)}, s32[]{:S(2)}) async-start(f32[2048]{0:T(1024)} %param.21, s32[]{:T(128)} %select_n.4), calls=%async_computation.10 | async-start | bytes 8704 | tf_op jit(solution)/shard_map/dynamic_slice | solution.py:103
Sparse Core Ops, SparseCore 0:
  9.5 51.7 all-gather.7
  63.4 47.6 all-gather.9
  113.1 48.8 all-gather.11
  165.0 5.9 reduce-scatter.2
  173.0 164.4 all-gather.13
  339.5 161.4 all-gather.15
  503.1 161.4 all-gather.17
  677.1 5.9 reduce-scatter.4
where the time goes:
time: 696 us; the launch traced here: 695 us
  waiting for transfers between devices  638 us (92%)
  matrix products  27 us (4%)
  between operations  13.6 us (2%)
  blocking collectives  11.7 us (2%)
    all_gather x1, waiting for transfers between devices, on_device(): lax.all_gather(ff_down, 'fs', axis=1, tiled=True)  164 us
    all_gather x1, waiting for transfers between devices, on_device(): lax.all_gather(ff_gate, 'fs', axis=0, tiled=True)  160 us
    all_gather x1, waiting for transfers between devices, on_device(): lax.all_gather(ff_up, 'fs', axis=0, tiled=True)  157 us
    all_gather x1, waiting for transfers between devices, on_device(): lax.all_gather(lin_weight, 'fs', axis=0, tiled=True)  50.2 us
    all_gather x1, waiting for transfers between devices, on_device(): lax.all_gather(glu_weight, 'fs', axis=0, tiled=True)  47.7 us
    all_gather x1, waiting for transfers between devices, on_device(): lax.all_gather(conv_out_weight, 'fs', axis=1, tiled=True)  44.9 us
  transfers between devices with their start and end apart: 8, of which 8 were waited for; matrix products, arithmetic and copies ran while one was open for 2% of the time, Pallas kernels for 0%

commit v1 on v0

--- a/solution.py
+++ b/solution.py
@@ -22,6 +22,18 @@
     return (values - average) * lax.rsqrt(second - average * average + epsilon)
 
 
+def exchange(blocks, axis):
+    return lax.all_to_all(blocks, axis, 0, 0)
+
+
+def after(value, *earlier):
+    return lax.optimization_barrier((value, *earlier))[0]
+
+
+def sum_blocks(blocks):
+    return jnp.sum(blocks.astype(jnp.float32), axis=0)
+
+
 def on_device(
     tokens,
     lin_weight,
@@ -35,19 +47,39 @@
     ff_down,
     out_gain,
 ):
+    n_fs = lax.axis_size("fs")
+    n_tp = lax.axis_size("tp")
     own_tokens = tokens[0]
-    feat_width = own_tokens.shape[1]
+    seq, feat_width = own_tokens.shape
     offset = lax.axis_index("tp") * feat_width
+    width = feat_width * n_tp
+    rows = lin_weight.shape[0]
+    chans = lin_weight.shape[1]
+    units = ff_gate.shape[1] // n_fs
+
     all_tokens = lax.all_gather(own_tokens, "tp", axis=1, tiled=True)
-    seq_rows = all_tokens.shape[0]
-    pieces = (
-        lax.all_gather(lin_weight, "fs", axis=0, tiled=True),
-        lax.all_gather(glu_weight, "fs", axis=0, tiled=True),
-    )
-    columns = all_tokens
-    linear = jnp.dot(columns, pieces[0], preferred_element_type=jnp.float32)
-    gating = jnp.dot(columns, pieces[1], preferred_element_type=jnp.float32)
-    glu = (linear * jax.nn.sigmoid(gating)).astype(jnp.bfloat16)
+    row_tokens = exchange(all_tokens.reshape(seq, n_fs, rows).transpose(1, 0, 2), "fs")
+    row_tokens = row_tokens.reshape(n_fs * seq, rows)
+
+    def dealt_columns(weight):
+        blocks = weight.reshape(rows, n_fs, units).transpose(1, 0, 2)
+        return exchange(blocks, "fs").reshape(n_fs * rows, units)
+
+    gate_own = dealt_columns(after(ff_gate, row_tokens))
+    up_own = dealt_columns(after(ff_up, row_tokens))
+
+    terms = jnp.concatenate(
+        [
+            jnp.dot(row_tokens, lin_weight, preferred_element_type=jnp.float32),
+            jnp.dot(row_tokens, glu_weight, preferred_element_type=jnp.float32),
+        ],
+        axis=1,
+    ).astype(jnp.bfloat16)
+    both = sum_blocks(exchange(terms.reshape(n_fs, seq, 2 * chans), "fs"))
+    down_blocks = after(ff_down, both).reshape(n_fs, units, ff_down.shape[1])
+    down_own = exchange(down_blocks, "fs").transpose(1, 0, 2).reshape(units, width)
+
+    glu = (both[:, :chans] * jax.nn.sigmoid(both[:, chans:])).astype(jnp.bfloat16)
     margin = (TAPS - 1) // 2
     conv = lax.conv_general_dilated(
         glu.astype(jnp.float32)[None],
@@ -78,26 +110,17 @@
     )
     gain_own = lax.dynamic_slice_in_dim(mix_gain, offset, feat_width, 0)
     middle_own = (scaled(before, mix_sums, mix_squares, D) * gain_own).astype(jnp.bfloat16)
-    middle_all = lax.all_gather(middle_own, "tp", axis=1, tiled=True)
-    empty_ffn = jnp.zeros((seq_rows, ff_gate.shape[1]), jnp.float32)
-    pieces = (
-        lax.all_gather(ff_gate, "fs", axis=0, tiled=True),
-        lax.all_gather(ff_up, "fs", axis=0, tiled=True),
-    )
-    columns = lax.slice_in_dim(middle_all, 0, pieces[0].shape[0], axis=1)
-    gate = empty_ffn + jnp.dot(columns, pieces[0], preferred_element_type=jnp.float32)
-    upward = empty_ffn + jnp.dot(columns, pieces[1], preferred_element_type=jnp.float32)
+
+    middle_half = lax.all_gather(middle_own, "fs", axis=0, tiled=True)
+    middle_all = lax.all_gather(middle_half, "tp", axis=1, tiled=True)
+    gate = jnp.dot(middle_all, gate_own, preferred_element_type=jnp.float32)
+    upward = jnp.dot(middle_all, up_own, preferred_element_type=jnp.float32)
     hidden = (jax.nn.silu(gate) * upward).astype(jnp.bfloat16)
-    down_terms = jnp.dot(
-        hidden,
-        lax.all_gather(ff_down, "fs", axis=1, tiled=True),
-        preferred_element_type=jnp.float32,
-    )
-    forward = rounded(
-        lax.psum_scatter(
-            down_terms.astype(jnp.bfloat16), "tp", scatter_dimension=1, tiled=True
-        ).astype(jnp.float32)
-    )
+    down_terms = jnp.dot(hidden, down_own, preferred_element_type=jnp.float32)
+    halves = down_terms.astype(jnp.bfloat16).reshape(n_fs * seq, n_tp, feat_width)
+    over_tp = sum_blocks(exchange(halves.transpose(1, 0, 2), "tp")).astype(jnp.bfloat16)
+    over_fs = sum_blocks(exchange(over_tp.reshape(n_fs, seq, feat_width), "fs"))
+    forward = rounded(over_fs)
     final = residual_scale * middle_own.astype(jnp.float32) + forward
     out_sums, out_squares = lax.psum((jnp.sum(final, axis=1), jnp.sum(final * final, axis=1)), "tp")
     gain_slice = lax.dynamic_slice_in_dim(out_gain, offset, feat_width, 0)

time: 696 us -> 261 us (0.38)
  waiting for transfers between devices: 638 us -> 168 us
  blocking collectives: 11.7 us -> 31.5 us
  starting transfers between devices: 0.27 us -> 18.9 us
  matrix products: 27 us -> 11.9 us
  local copies, waits for them, and re-layouts: 0.04 us -> 9.7 us
    all_gather x5 -> x2, waiting for transfers between devices: 579 us -> 25.7 us  [the longest x1 25.7 us: on_device(): middle_half = lax.all_gather(middle_own, 'fs', axis=0, tiled=True)]
    all_to_all x0 -> x5, waiting for transfers between devices: none -> 132 us  [exchange(): return lax.all_to_all(blocks, axis, 0, 0)]
    all_gather x1, waiting for transfers between devices: 44.9 us -> 0.02 us  [on_device(): lax.all_gather(conv_out_weight, 'fs', axis=1, tiled=True)]
    all_to_all x0 -> x2, blocking collectives: none -> 21.6 us  [exchange(): return lax.all_to_all(blocks, axis, 0, 0)]
    all_to_all x0 -> x5, starting transfers between devices: none -> 18.7 us  [exchange(): return lax.all_to_all(blocks, axis, 0, 0)]
    dot_general x4, matrix products: 22.9 us -> 7.74 us  [the longest x1 4.63 us: on_device(): down_terms = jnp.dot(hidden, down_own, preferred_element_type=jnp.float32)]
  transfers between devices with their start and end apart: 8 -> 9, of which waited for: 8 -> 7; matrix products, arithmetic and copies ran while one was open for 2% -> 6% of each run, Pallas kernels for 0% -> 0%
where the time goes in v1:
time: 261 us; the launch traced here: 260 us
  waiting for transfers between devices  168 us (64%)
  blocking collectives  31.5 us (12%)
  starting transfers between devices  18.9 us (7%)
  between operations  13.4 us (5%)
  matrix products  11.9 us (5%)
  local copies, waits for them, and re-layouts  9.7 us (4%)
  other arithmetic  7.01 us (3%)
    all_to_all x5, waiting for transfers between devices, exchange(): return lax.all_to_all(blocks, axis, 0, 0)  132 us
    all_gather x1, waiting for transfers between devices, on_device(): middle_half = lax.all_gather(middle_own, 'fs', axis=0, tiled=True)  25.7 us
    all_to_all x2, blocking collectives, exchange(): return lax.all_to_all(blocks, axis, 0, 0)  21.6 us
    all_to_all x5, starting transfers between devices, exchange(): return lax.all_to_all(blocks, axis, 0, 0)  18.7 us
    reduce_scatter x1, waiting for transfers between devices, on_device(): lax.psum_scatter(conv_terms.astype(jnp.bfloat16), 'tp', scatter_dimension...  9.16 us
  transfers between devices with their start and end apart: 9, of which 7 were waited for; matrix products, arithmetic and copies ran while one was open for 6% of the time, Pallas kernels for 0%

profile of v1, /device:TPU:0, one launch (start us, length us, event | category | flops | bytes accessed | tf_op | source)
XLA Modules:
  0.0 260.5 jit_solution(7943047915175370196)
XLA Ops:
  6.5 2.5 all-gather
  9.1 16.2 %all_to_all.35 = bf16[8,64,256]{2,1,0:T(8,128)(2,1)S(1)} all-to-all(bf16[8,64,256]{2,1,0:T(8,128)(2,1)S(1)} %bitcast.77), channel_id=1, replica_groups=mesh['rep'=2,'fs'=8,'tp'=2] {'fs'}, dimensions={0} | all-to-all | bytes 524288 | tf_op jit(solution)/shard_map/all_to_all | solution.py:26
  27.1 3.6 %all-to-all-start.1 = ((bf16[8,64,1024]{2,1,0:T(8,128)(2,1)}), bf16[8,64,1024]{2,1,0:T(8,128)(2,1)S(1)}, u32[]{:S(2)}, u32[]{:S(2)}) async-start(bf16[8,64,1024]{2,1,0:T(8,128)(2,1)} %pad_maximum_fusion), calls=%async_computation.1 | async-start | bytes 2097152 | tf_op jit(solution)/shard_map/all_to_all | solution.py:26
  32.9 31.7 %all-to-all-done.1 = bf16[8,64,1024]{2,1,0:T(8,128)(2,1)S(1)} async-done(((bf16[8,64,1024]{2,1,0:T(8,128)(2,1)}), bf16[8,64,1024]{2,1,0:T(8,128)(2,1)S(1)}, u32[]{:S(2)}, u32[]{:S(2)}) %all-to-all-start.1) | async-done | bytes 1048608 | tf_op jit(solution)/shard_map/all_to_all | solution.py:26
  64.7 3.6 %all-to-all-start.2 = ((bf16[8,256,352]{1,2,0:T(8,128)(2,1)}), bf16[8,256,352]{1,2,0:T(8,128)(2,1)S(1)}, u32[]{:S(2)}, u32[]{:S(2)}) async-start(bf16[8,256,352]{1,2,0:T(8,128)(2,1)} %bitcast.8), calls=%async_computation.3 | async-start | bytes 2883584 | tf_op jit(solution)/shard_map/all_to_all | solution.py:26
  68.3 2.6 copy.36
  72.5 2.5 all-reduce.2
  75.0 42.4 %all-to-all-done.2 = bf16[8,256,352]{1,2,0:T(8,128)(2,1)S(1)} async-done(((bf16[8,256,352]{1,2,0:T(8,128)(2,1)}), bf16[8,256,352]{1,2,0:T(8,128)(2,1)S(1)}, u32[]{:S(2)}, u32[]{:S(2)}) %all-to-all-start.2) | async-done | bytes 1441824 | tf_op jit(solution)/shard_map/all_to_all | solution.py:26
  117.4 3.6 %all-to-all-start.3 = ((bf16[8,256,352]{1,2,0:T(8,128)(2,1)}), bf16[8,256,352]{1,2,0:T(8,128)(2,1)S(1)}, u32[]{:S(2)}, u32[]{:S(2)}) async-start(bf16[8,256,352]{1,2,0:T(8,128)(2,1)} %bitcast.10), calls=%async_computation.4 | async-start | bytes 2883584 | tf_op jit(solution)/shard_map/all_to_all | solution.py:26
  121.1 2.9 %convolution_convert_fusion.1 = bf16[64,2048]{1,0:T(8,128)(2,1)} fusion(bf16[512,2048]{1,0:T(8,128)(2,1)} %all-gather.5.cloned.1.call-done, f32[1,64,512]{2,0,1:T(1,128)S(1)} %get-tuple-element.28, f32[512]{0:T(512)S(1)} %copy-done.7, f32[64]{0:T(128)S(1)} %get-tuple-element.26, f32[64]{0:T(128)S(1)} %get-tuple-element.25), kind=kOutput, calls=%fused_computation.1 | convolution fusion | flops 134610944 | bytes 2492928 | tf_op jit(solution)/shard_map/dot_general | solution.py:97
  124.0 9.2 %reduce-scatter.2.cloned.1.call-done = bf16[64,1024]{1,0:T(8,128)(2,1)} async-done(((bf16[64,2048]{1,0:T(8,128)(2,1)}), bf16[64,1024]{1,0:T(8,128)(2,1)}) %reduce-scatter.2.cloned.1.call-update) | async-done | bytes 131088 | tf_op jit(solution)/shard_map/reduce_scatter | solution.py:103
  134.3 2.5 all-reduce.1
  138.4 18.6 %all-to-all-done.3 = bf16[8,256,352]{1,2,0:T(8,128)(2,1)S(1)} async-done(((bf16[8,256,352]{1,2,0:T(8,128)(2,1)}), bf16[8,256,352]{1,2,0:T(8,128)(2,1)S(1)}, u32[]{:S(2)}, u32[]{:S(2)}) %all-to-all-start.3) | async-done | bytes 1441824 | tf_op jit(solution)/shard_map/all_to_all | solution.py:26
  157.0 4.3 %all-to-all-start.4 = ((bf16[8,352,256]{2,1,0:T(8,128)(2,1)}), bf16[8,352,256]{2,1,0:T(8,128)(2,1)}, u32[]{:S(2)}, u32[]{:S(2)}) async-start(bf16[8,352,256]{2,1,0:T(8,128)(2,1)} %bitcast.72), calls=%async_computation.5 | async-start | bytes 2883584 | tf_op jit(solution)/shard_map/all_to_all | solution.py:26
  161.3 25.7 %all-gather.7.cloned.1.call-done = bf16[512,1024]{1,0:T(8,128)(2,1)} async-done(((bf16[64,1024]{1,0:T(8,128)(2,1)}), bf16[512,1024]{1,0:T(8,128)(2,1)}) %all-gather.7.cloned.1.call-update) | async-done | bytes 1048592 | tf_op jit(solution)/shard_map/all_gather | solution.py:114
  189.7 13.6 %all-to-all-done.4 = bf16[8,352,256]{2,1,0:T(8,128)(2,1)} async-done(((bf16[8,352,256]{2,1,0:T(8,128)(2,1)}), bf16[8,352,256]{2,1,0:T(8,128)(2,1)}, u32[]{:S(2)}, u32[]{:S(2)}) %all-to-all-start.4) | async-done | bytes 1441824 | tf_op jit(solution)/shard_map/all_to_all | solution.py:26
  203.3 2.7 %copy.44 = bf16[8,44,8,256]{3,2,0,1:T(8,128)(2,1)} copy(bf16[8,44,8,256]{3,2,1,0:T(8,128)(2,1)} %bitcast.25) | data formatting | bytes 2883584 | tf_op jit(solution)/shard_map/reshape | solution.py:80
  205.9 2.5 fusion.31
  208.5 4.6 %convolution_convert_fusion = bf16[512,2048]{1,0:T(8,128)(2,1)S(1)} fusion(bf16[352,2048]{1,0:T(8,128)(2,1)} %bitcast.75, bf16[512,2048]{1,0:T(8,128)(2,1)} %all-gather.9.cloned.1.call-done, bf16[2048,352]{0,1:T(8,128)(2,1)} %bitcast.73, f32[512,352]{0,1:T(8,128)S(1)} %fusion.31), kind=kOutput, calls=%fused_computation | convolution fusion | flops 1478524928 | bytes 7798784 | tf_op jit(solution)/shard_map/dot_general | solution.py:119
  213.3 5.4 %all_to_all.36 = bf16[2,512,1024]{2,1,0:T(8,128)(2,1)S(1)} all-to-all(bf16[2,512,1024]{2,1,0:T(8,128)(2,1)S(1)} %bitcast.68), channel_id=1, replica_groups=mesh['rep'=2,'fs'=8,'tp'=2] {'tp'}, dimensions={0} | all-to-all | bytes 4194304 | tf_op jit(solution)/shard_map/all_to_all | solution.py:26
  218.7 1.7 reduce_sum.92
  220.4 3.7 %all-to-all-start.6 = ((bf16[8,64,1024]{2,1,0:T(8,128)(2,1)}), bf16[8,64,1024]{2,1,0:T(8,128)(2,1)S(1)}, u32[]{:S(2)}, u32[]{:S(2)}) async-start(bf16[8,64,1024]{2,1,0:T(8,128)(2,1)} %bitcast.14), calls=%async_computation.7 | async-start | bytes 2097152 | tf_op jit(solution)/shard_map/all_to_all | solution.py:26
  224.1 26.3 %all-to-all-done.6 = bf16[8,64,1024]{2,1,0:T(8,128)(2,1)S(1)} async-done(((bf16[8,64,1024]{2,1,0:T(8,128)(2,1)}), bf16[8,64,1024]{2,1,0:T(8,128)(2,1)S(1)}, u32[]{:S(2)}, u32[]{:S(2)}) %all-to-all-start.6) | async-done | bytes 1048608 | tf_op jit(solution)/shard_map/all_to_all | solution.py:26
  250.7 2.5 all-reduce
  (52 shorter events, 12.6 us)
Async XLA Ops:
  6.5 18.8 %copy-start = (bf16[256,512]{1,0:T(8,128)(2,1)S(1)}, bf16[256,512]{1,0:T(8,128)(2,1)}, u32[]{:S(2)}) copy-start(bf16[256,512]{1,0:T(8,128)(2,1)} %param.13) | copy-start | bytes 786436
  6.5 19.1 %copy-start.5 = (bf16[256,512]{1,0:T(8,128)(2,1)S(1)}, bf16[256,512]{1,0:T(8,128)(2,1)}, u32[]{:S(2)}) copy-start(bf16[256,512]{1,0:T(8,128)(2,1)} %param.12) | copy-start | bytes 786436
  25.9 5.5 %copy-start.2 = (bf16[256,2816]{1,0:T(8,128)(2,1)S(1)}, bf16[256,2816]{1,0:T(8,128)(2,1)}, u32[]{:S(2)}) copy-start(bf16[256,2816]{1,0:T(8,128)(2,1)} %param.18) | copy-start | bytes 4325380
  27.1 37.6 %all-to-all-start.1 = ((bf16[8,64,1024]{2,1,0:T(8,128)(2,1)}), bf16[8,64,1024]{2,1,0:T(8,128)(2,1)S(1)}, u32[]{:S(2)}, u32[]{:S(2)}) async-start(bf16[8,64,1024]{2,1,0:T(8,128)(2,1)} %pad_maximum_fusion), calls=%async_computation.1 | async-start | bytes 2097152 | tf_op jit(solution)/shard_map/all_to_all | solution.py:26
  30.6 90.4 %all-gather.5.cloned.1.call-start = ((), (), s32[]{:S(2)}) async-start(), calls=%async_computation.8 | async-start | bytes 2359296 | tf_op jit(solution)/shard_map/all_gather | solution.py:99
  64.7 52.7 %all-to-all-start.2 = ((bf16[8,256,352]{1,2,0:T(8,128)(2,1)}), bf16[8,256,352]{1,2,0:T(8,128)(2,1)S(1)}, u32[]{:S(2)}, u32[]{:S(2)}) async-start(bf16[8,256,352]{1,2,0:T(8,128)(2,1)} %bitcast.8), calls=%async_computation.3 | async-start | bytes 2883584 | tf_op jit(solution)/shard_map/all_to_all | solution.py:26
  68.3 2.8 %copy-start.8 = (f32[31,512]{1,0:T(8,128)S(1)}, f32[31,512]{1,0:T(8,128)}, u32[]{:S(2)}) copy-start(f32[31,512]{1,0:T(8,128)} %param.14) | copy-start | bytes 190468
  71.1 50.0 %copy-start.7 = (f32[512]{0:T(512)S(1)}, f32[512]{0:T(512)}, u32[]{:S(2)}) copy-start(f32[512]{0:T(512)} %param.15) | copy-start | bytes 6148
  117.4 39.6 %all-to-all-start.3 = ((bf16[8,256,352]{1,2,0:T(8,128)(2,1)}), bf16[8,256,352]{1,2,0:T(8,128)(2,1)S(1)}, u32[]{:S(2)}, u32[]{:S(2)}) async-start(bf16[8,256,352]{1,2,0:T(8,128)(2,1)} %bitcast.10), calls=%async_computation.4 | async-start | bytes 2883584 | tf_op jit(solution)/shard_map/all_to_all | solution.py:26
  121.0 3.0 %copy-start.6 = (f32[2048]{0:T(1024)S(1)}, f32[2048]{0:T(1024)}, u32[]{:S(2)}) copy-start(f32[2048]{0:T(1024)} %param.17) | copy-start | bytes 24580
  121.0 12.2 %copy-start.4 = (bf16[1,64,1024]{2,1,0:T(8,128)(2,1)S(1)}, bf16[1,64,1024]{2,1,0:T(8,128)(2,1)}, u32[]{:S(2)}) copy-start(bf16[1,64,1024]{2,1,0:T(8,128)(2,1)} %param.11) | copy-start | bytes 393220
  121.0 12.2 %reduce-scatter.2.cloned.1.call-start = ((), (), s32[]{:S(2)}) async-start(), calls=%async_computation.9 | async-start | bytes 393216 | tf_op jit(solution)/shard_map/reduce_scatter | solution.py:103
  123.9 63.2 %all-gather.7.cloned.1.call-start = ((), (), s32[]{:S(2)}) async-start(), calls=%async_computation.10 | async-start | bytes 1179648 | tf_op jit(solution)/shard_map/all_gather | solution.py:114
  157.0 46.3 %all-to-all-start.4 = ((bf16[8,352,256]{2,1,0:T(8,128)(2,1)}), bf16[8,352,256]{2,1,0:T(8,128)(2,1)}, u32[]{:S(2)}, u32[]{:S(2)}) async-start(bf16[8,352,256]{2,1,0:T(8,128)(2,1)} %bitcast.72), calls=%async_computation.5 | async-start | bytes 2883584 | tf_op jit(solution)/shard_map/all_to_all | solution.py:26
  161.3 44.6 %all-gather.9.cloned.1.call-start = ((), (), s32[]{:S(2)}) async-start(), calls=%async_computation.11 | async-start | bytes 3145728 | tf_op jit(solution)/shard_map/all_gather | solution.py:115
  189.7 16.2 %copy-start.3 = (bf16[8,44,8,256]{3,2,0,1:T(8,128)(2,1)S(1)}, bf16[8,44,8,256]{3,2,0,1:T(8,128)(2,1)}, u32[]{:S(2)}) copy-start(bf16[8,44,8,256]{3,2,0,1:T(8,128)(2,1)} %copy.42) | copy-start | bytes 4325380
  220.4 30.1 %copy-start.1 = (bf16[64,1024]{1,0:T(8,128)(2,1)S(1)}, bf16[64,1024]{1,0:T(8,128)(2,1)}, u32[]{:S(2)}) copy-start(bf16[64,1024]{1,0:T(8,128)(2,1)} %multiply_convert_fusion.1) | copy-start | bytes 393220
  220.4 32.8 %dynamic-slice-start = ((f32[2048]{0:T(1024)}, s32[]{:T(128)}), f32[1024]{0:T(1024)S(1)}, s32[]{:S(2)}) async-start(f32[2048]{0:T(1024)} %param.21, s32[]{:T(128)} %select_n.4), calls=%async_computation.12 | async-start | bytes 8704 | tf_op jit(solution)/shard_map/dynamic_slice | solution.py:126
  220.4 30.0 %all-to-all-start.6 = ((bf16[8,64,1024]{2,1,0:T(8,128)(2,1)}), bf16[8,64,1024]{2,1,0:T(8,128)(2,1)S(1)}, u32[]{:S(2)}, u32[]{:S(2)}) async-start(bf16[8,64,1024]{2,1,0:T(8,128)(2,1)} %bitcast.14), calls=%async_computation.7 | async-start | bytes 2097152 | tf_op jit(solution)/shard_map/all_to_all | solution.py:26
Sparse Core Ops, SparseCore 0:
  33.5 80.9 all-gather.4
  124.1 9.0 reduce-scatter.1
  138.5 48.5 all-gather.6
  188.5 14.5 all-gather.8
